TPU v7x, 32 devices: a whole 2x2x4 slice. The times are simulated.
32 devices in a mesh: sp: 8 (over z, x), dp: 4 (over y, core).
Axes of the slice: x: 2, y: 2, z: 4, core: 2. Of those that a mesh axis runs over, the one named last changes fastest.
Arguments:
- activations: bfloat16 [4, 4096, 2048], P('dp', 'sp'), may hold values from -6 to 6
- value_weight: bfloat16 [2048, 1024], P(('sp', 'dp')), may hold values from -0.125 to 0.125
- gate_weight: bfloat16 [2048, 1024], P(('sp', 'dp')), may hold values from -0.125 to 0.125
- input_weight: bfloat16 [2048, 512], P(('sp', 'dp')), may hold values from -0.125 to 0.125
- readout_weight: bfloat16 [2048, 512], P(('sp', 'dp')), may hold values from -0.125 to 0.125
- rate_weight: bfloat16 [2048, 16], replicated, may hold values from -0.125 to 0.125
- value_taps: bfloat16 [4, 1024], replicated, may hold values from -0.375 to 0.375
- input_taps: bfloat16 [4, 512], replicated, may hold values from -3 to 3
- readout_taps: bfloat16 [4, 512], replicated, may hold values from -3 to 3
- rate_bias: float32 [16], replicated, may hold values from -1 to 1
- decay_log: float32 [16], replicated, may hold values from -1 to 1.5
- norm_gain: float32 [1024], replicated, may hold values from 0.1 to 1.9
- out_weight: bfloat16 [1024, 2048], P(None, ('sp', 'dp')), may hold values from -0.1875 to 0.1875
Outputs:
- mixed_out: bfloat16 [4, 4096, 2048], P('dp', 'sp')
All inputs are finite; a program needn't handle non-finite values.
Results may differ from a plain program's by a relative error of at most 0.014.
Values may be sent and summed in bfloat16 or wider, within the bound.
No kernel may reach another device: no remote copies, remote signals or barrier semaphores. Data moves between devices by JAX's collectives and lax.ppermute only.
A program may use at most 128 MiB of HBM per device.

v0:
```python
import jax
import jax.numpy as jnp
from jax import lax
from jax.sharding import PartitionSpec as P

HEADS = 16
HEAD_DIM = 64
GROUPS = 4
STATE = 128
BLOCK = 64


norm_eps = 1.0


def broaden(matrix, groups, head_count):
    row_count = matrix.shape[0]
    group_width = matrix.shape[1] // groups
    spread = matrix.reshape(row_count, groups, 1, group_width)
    spread = jnp.broadcast_to(spread, (row_count, groups, head_count // groups, group_width))
    return spread.reshape(row_count, head_count * group_width)


def extended_conv(before, series, kernel):
    extent = kernel.shape[0]
    length = series.shape[0]
    padded = jnp.concatenate([before, series], axis=0).astype(jnp.float32)
    result = jnp.zeros(series.shape, jnp.float32)
    for offset in range(extent):
        result = result + kernel[offset].astype(jnp.float32) * padded[offset : offset + length]
    return result


def causal_conv(series, kernel):
    before = jnp.zeros((kernel.shape[0] - 1, series.shape[1]), series.dtype)
    return extended_conv(before, series, kernel)


def block_parts(values, inputs, readouts, rates, decay):
    length, head_count, head_width = values.shape
    blocks = length // BLOCK
    block_values = values.reshape(blocks, BLOCK, head_count, head_width)
    block_inputs = inputs.reshape(blocks, BLOCK, head_count, -1)
    block_reads = readouts.reshape(blocks, BLOCK, head_count, -1)
    block_rates = rates.reshape(blocks, BLOCK, head_count)
    running = jnp.cumsum(block_rates * decay, axis=1)
    by_head = jnp.transpose(running, (0, 2, 1))
    rate_head = jnp.transpose(block_rates, (0, 2, 1))
    causal = jnp.tril(jnp.ones((BLOCK, BLOCK), dtype=bool))
    intervals = by_head[:, :, :, None] - by_head[:, :, None, :]
    fading = jnp.where(causal, jnp.exp(jnp.minimum(intervals, 0.0)), 0.0)
    intersect = jnp.einsum(
        "bthn,bshn->bhts", block_reads, block_inputs, preferred_element_type=jnp.float32
    )
    scores = (intersect * fading * rate_head[:, :, None, :]).astype(jnp.bfloat16)
    within = jnp.einsum("bhts,bshp->bthp", scores, block_values, preferred_element_type=jnp.float32)
    tail_fade = jnp.exp(running[:, -1:, :] - running) * block_rates
    weighted = (block_values.astype(jnp.float32) * tail_fade[:, :, :, None]).astype(jnp.bfloat16)
    states = jnp.einsum(
        "bshp,bshn->bhpn", weighted, block_inputs, preferred_element_type=jnp.float32
    )
    return (within, states, running, block_reads)


def finish(within, states, running, block_reads, initial):
    blocks, block_len, head_count, head_width = within.shape
    totals = jnp.cumsum(running[:, -1, :], axis=0)
    starts = totals - running[:, -1, :]
    earlier = jnp.tril(jnp.ones((blocks, blocks), dtype=bool), -1)
    carried = jnp.where(
        earlier[:, :, None], jnp.exp(jnp.minimum(starts[:, None, :] - totals[None, :, :], 0.0)), 0.0
    )
    entering = jnp.einsum("cdh,dhpn->chpn", carried, states, precision=lax.Precision.HIGHEST)
    entering = entering + jnp.exp(starts)[:, :, None, None] * initial[None]
    across = jnp.einsum(
        "bthn,bhpn->bthp",
        block_reads.astype(jnp.float32),
        entering,
        precision=lax.Precision.HIGHEST,
    )
    across = across * jnp.exp(running)[:, :, :, None]
    return (within + across).reshape(blocks * block_len, head_count * head_width)


def per_device(
    activations,
    value_weight,
    gate_weight,
    input_weight,
    readout_weight,
    rate_weight,
    value_taps,
    input_taps,
    readout_taps,
    rate_bias,
    decay_log,
    norm_gain,
    out_weight,
):
    sequence = activations[0]

    def add_rows(piece):
        return jnp.dot(sequence, piece, preferred_element_type=jnp.float32)

    rate_raw = jnp.dot(sequence, rate_weight, preferred_element_type=jnp.float32).astype(
        jnp.bfloat16
    )
    pieces = (
        lax.all_gather(value_weight, ("sp", "dp"), axis=0, tiled=True),
        lax.all_gather(gate_weight, ("sp", "dp"), axis=0, tiled=True),
        lax.all_gather(input_weight, ("sp", "dp"), axis=0, tiled=True),
        lax.all_gather(readout_weight, ("sp", "dp"), axis=0, tiled=True),
    )
    value_sum, gate_sum, input_sum, readout_sum = tuple((add_rows(piece) for piece in pieces))
    gate_proj = gate_sum.astype(jnp.bfloat16)
    wide_inputs = broaden(input_sum.astype(jnp.bfloat16), GROUPS, HEADS)
    wide_reads = broaden(readout_sum.astype(jnp.bfloat16), GROUPS, HEADS)
    head_values, head_inputs, head_reads, head_rates = (
        lax.all_to_all(
            value_sum.astype(jnp.bfloat16), "sp", split_axis=1, concat_axis=0, tiled=True
        ),
        lax.all_to_all(wide_inputs, "sp", split_axis=1, concat_axis=0, tiled=True),
        lax.all_to_all(wide_reads, "sp", split_axis=1, concat_axis=0, tiled=True),
        lax.all_to_all(rate_raw, "sp", split_axis=1, concat_axis=0, tiled=True),
    )
    length = head_values.shape[0]
    local_heads = head_rates.shape[1]
    first = lax.axis_index("sp") * local_heads
    value_kernel = lax.dynamic_slice_in_dim(value_taps, first * HEAD_DIM, local_heads * HEAD_DIM, 1)
    input_kernel = lax.dynamic_slice_in_dim(
        broaden(input_taps, GROUPS, HEADS), first * STATE, local_heads * STATE, 1
    )
    readout_kernel = lax.dynamic_slice_in_dim(
        broaden(readout_taps, GROUPS, HEADS), first * STATE, local_heads * STATE, 1
    )
    conv_values = jax.nn.silu(causal_conv(head_values, value_kernel)).astype(jnp.bfloat16)
    conv_inputs = jax.nn.silu(causal_conv(head_inputs, input_kernel)).astype(jnp.bfloat16)
    conv_reads = jax.nn.silu(causal_conv(head_reads, readout_kernel)).astype(jnp.bfloat16)
    local_bias = lax.dynamic_slice_in_dim(rate_bias, first, local_heads, 0)
    rates = jax.nn.softplus(head_rates.astype(jnp.float32) + local_bias)
    decay = -jnp.exp(lax.dynamic_slice_in_dim(decay_log, first, local_heads, 0)) / length
    within, states, running, block_reads = block_parts(
        conv_values.reshape(length, local_heads, HEAD_DIM),
        conv_inputs.reshape(length, local_heads, STATE),
        conv_reads.reshape(length, local_heads, STATE),
        rates,
        decay,
    )
    initial = jnp.zeros((local_heads, HEAD_DIM, STATE), jnp.float32)
    mixed = finish(within, states, running, block_reads, initial).astype(jnp.bfloat16)
    returned = lax.all_to_all(mixed, "sp", split_axis=0, concat_axis=1, tiled=True)
    gated = returned.astype(jnp.float32) * jax.nn.silu(gate_proj.astype(jnp.float32))
    scale = lax.rsqrt(jnp.mean(gated * gated, axis=-1, keepdims=True) + norm_eps)
    normed = (gated * scale * norm_gain).astype(jnp.bfloat16)
    result = jnp.dot(
        normed,
        lax.all_gather(out_weight, ("sp", "dp"), axis=1, tiled=True),
        preferred_element_type=jnp.float32,
    )
    return result.astype(jnp.bfloat16)[None]


def solution(mesh):
    placed = (
        P("dp", "sp", None),
        P(("sp", "dp"), None),
        P(("sp", "dp"), None),
        P(("sp", "dp"), None),
        P(("sp", "dp"), None),
        P(),
        P(),
        P(),
        P(),
        P(),
        P(),
        P(),
        P(None, ("sp", "dp")),
    )
    return jax.shard_map(
        per_device, mesh=mesh, in_specs=placed, out_specs=P("dp", "sp", None), check_vma=False
    )
```

profile of v0, /device:TPU:29, one launch (start us, length us, event | category | flops | bytes accessed | tf_op | source)
XLA Modules:
  0.0 389.0 jit_solution(17978753854210989949)
XLA Ops:
  6.5 0.7 all-gather.10.cloned.1.call-update
  9.3 1.5 fusion.56
  11.4 5.5 %all-to-all-start.3 = ((bf16[512,8,2]{0,2,1:T(2,128)(2,1)}), bf16[512,8,2]{0,2,1:T(2,128)(2,1)S(1)}, u32[]{:S(2)}, u32[]{:S(2)}) async-start(bf16[512,8,2]{0,2,1:T(2,128)(2,1)} %all_to_all.72), calls=%async_computation.3 | async-start | bytes 32768 | tf_op jit(solution)/shard_map/all_to_all | solution.py:124
  16.9 49.7 %all-gather.10.cloned.1.call-done = bf16[2048,512]{1,0:T(8,128)(2,1)} async-done(((bf16[64,512]{1,0:T(8,128)(2,1)}), bf16[2048,512]{1,0:T(8,128)(2,1)}) %all-gather.10.cloned.1.call-update) | async-done | bytes 2097168 | tf_op jit(solution)/shard_map/all_gather | solution.py:111
  66.6 2.9 fusion.53
  69.5 1.5 broadcast_in_dim.41
  71.1 5.6 %all-to-all-start.2 = ((bf16[512,8,256]{0,2,1:T(8,128)(2,1)}), bf16[512,8,256]{0,2,1:T(8,128)(2,1)}, u32[]{:S(2)}, u32[]{:S(2)}) async-start(bf16[512,8,256]{0,2,1:T(8,128)(2,1)} %bitcast.114), calls=%async_computation.2 | async-start | bytes 4194304 | tf_op jit(solution)/shard_map/all_to_all | solution.py:122
  78.0 70.5 %all-gather.8.cloned.1.call-done = bf16[2048,512]{1,0:T(8,128)(2,1)} async-done(((bf16[64,512]{1,0:T(8,128)(2,1)}), bf16[2048,512]{1,0:T(8,128)(2,1)}) %all-gather.8.cloned.1.call-update) | async-done | bytes 2097168 | tf_op jit(solution)/shard_map/all_gather | solution.py:112
  148.5 2.9 fusion.50
  151.4 1.5 broadcast_in_dim.36
  152.9 6.0 %all-to-all-start.1 = ((bf16[512,8,256]{0,2,1:T(8,128)(2,1)}), bf16[512,8,256]{0,2,1:T(8,128)(2,1)}, u32[]{:S(2)}, u32[]{:S(2)}) async-start(bf16[512,8,256]{0,2,1:T(8,128)(2,1)} %bitcast.113), calls=%async_computation.1 | async-start | bytes 4194304 | tf_op jit(solution)/shard_map/all_to_all | solution.py:123
  159.6 2.9 copy.120
  162.5 1.7 fusion.78
  164.3 1.3 copy-done.1
  165.6 2.6 copy.126
  168.2 3.3 exp.63
  172.2 2.7 copy.137
  174.9 2.7 copy.121
  177.5 3.9 %copy.116 = bf16[8,512,256]{2,1,0:T(8,128)(2,1)} copy(bf16[8,512,256]{1,2,0:T(8,128)(2,1)} %bitcast.18) | data formatting | bytes 4194304 | tf_op jit(solution)/shard_map/all_to_all | solution.py:122
  181.4 2.0 pad_convert_fusion
  183.4 3.6 multiply_convert_fusion.2
  187.0 4.0 %reshape_reshape.11 = bf16[64,64,2,128]{3,2,1,0:T(2,128)(2,1)} reshape(bf16[4096,256]{1,0:T(8,128)(2,1)} %multiply_convert_fusion.2) | data formatting | bytes 4194304 | tf_op jit(solution)/shard_map/reshape;reshape | solution.py:43
  191.1 22.7 %all-to-all-done.1 = bf16[512,8,256]{0,2,1:T(8,128)(2,1)} async-done(((bf16[512,8,256]{0,2,1:T(8,128)(2,1)}), bf16[512,8,256]{0,2,1:T(8,128)(2,1)}, u32[]{:S(2)}, u32[]{:S(2)}) %all-to-all-start.1) | async-done | bytes 2097184 | tf_op jit(solution)/shard_map/all_to_all | solution.py:123
  213.7 3.9 %copy.115 = bf16[8,512,256]{2,1,0:T(8,128)(2,1)} copy(bf16[8,512,256]{1,2,0:T(8,128)(2,1)} %bitcast.10) | data formatting | bytes 4194304 | tf_op jit(solution)/shard_map/all_to_all | solution.py:123
  217.6 19.5 %all-gather.6.cloned.1.call-done = bf16[2048,1024]{1,0:T(8,128)(2,1)} async-done(((bf16[64,1024]{1,0:T(8,128)(2,1)}), bf16[2048,1024]{1,0:T(8,128)(2,1)}) %all-gather.6.cloned.1.call-update) | async-done | bytes 4194320 | tf_op jit(solution)/shard_map/all_gather | solution.py:109
  237.1 4.5 %fusion.47 = bf16[64,8,8,128]{3,2,1,0:T(8,128)(2,1)S(1)} fusion(bf16[2048,1024]{1,0:T(8,128)(2,1)} %all-gather.6.cloned.1.call-done, bf16[1,512,2048]{2,1,0:T(8,128)(2,1)S(1)} %copy-done), kind=kOutput, calls=%fused_computation.65 | convolution fusion | flops 2148007936 | bytes 7340032 | tf_op jit(solution)/shard_map/dot_general | solution.py:103
  241.7 1.2 copy.168
  242.9 5.2 %all-to-all-start = ((bf16[512,8,128]{2,0,1:T(8,128)(2,1)}), bf16[512,8,128]{2,0,1:T(8,128)(2,1)S(1)}, u32[]{:S(2)}, u32[]{:S(2)}) async-start(bf16[512,8,128]{2,0,1:T(8,128)(2,1)} %bitcast.119), calls=%async_computation | async-start | bytes 2097152 | tf_op jit(solution)/shard_map/all_to_all | solution.py:119
  248.1 2.0 pad_convert_fusion.1
  250.1 3.6 multiply_convert_fusion.3
  253.7 4.0 %reshape_reshape.10 = bf16[64,64,2,128]{3,2,1,0:T(2,128)(2,1)} reshape(bf16[4096,256]{1,0:T(8,128)(2,1)} %multiply_convert_fusion.3) | data formatting | bytes 4194304 | tf_op jit(solution)/shard_map/reshape;reshape | solution.py:44
  257.7 18.6 %all-to-all-done = bf16[512,8,128]{2,0,1:T(8,128)(2,1)S(1)} async-done(((bf16[512,8,128]{2,0,1:T(8,128)(2,1)}), bf16[512,8,128]{2,0,1:T(8,128)(2,1)S(1)}, u32[]{:S(2)}, u32[]{:S(2)}) %all-to-all-start) | async-done | bytes 1048608 | tf_op jit(solution)/shard_map/all_to_all | solution.py:119
  276.5 1.3 multiply_convert_fusion.5
  277.8 1.4 copy.114
  279.2 4.2 %reshape_reshape.9 = bf16[64,64,2,64]{1,0,3,2:T(8,128)(2,1)} reshape(bf16[4096,128]{0,1:T(8,128)(2,1)} %copy.114) | data formatting | bytes 2097152 | tf_op jit(solution)/shard_map/reshape;reshape | solution.py:42
  283.4 2.4 multiply_convert_fusion
  285.8 2.6 fusion.32
  288.4 6.7 %bitcast_add_fusion = f32[64,2,64,128]{3,0,2,1:T(8,128)S(1)} fusion(f32[64,2,64,128]{3,2,1,0:T(8,128)S(1)} %fusion.32, f32[64,2]{0,1:T(2,128)S(1)} %copy.134, f32[64,2]{0,1:T(2,128)S(1)} %copy.130, f32[64,2]{0,1:T(2,128)S(1)} %fusion.74, pred[64,64]{1,0:T(8,128)(4,1)S(1)} %iota_compare_fusion), kind=kOutput, calls=%fused_computation.17 | convolution fusion | flops 806379520 | bytes 8394240 | tf_op jit(solution)/shard_map/cdh,dhpn->chpn/dot_general | solution.py:73
  295.0 8.6 %fusion.8 = f32[64,2,64,64]{3,2,1,0:T(8,128)} fusion(f32[64,2,64,128]{3,0,2,1:T(8,128)S(1)} %bitcast_add_fusion, bf16[64,64,2,128]{3,2,1,0:T(2,128)(2,1)S(1)} %copy-done.2), kind=kOutput, calls=%fused_computation.18 | convolution fusion | flops 805306368 | bytes 8388608 | tf_op jit(solution)/shard_map/bthn,bhpn->bthp/dot_general | solution.py:75
  303.7 7.3 %fusion.7 = bf16[64,64,2,64]{1,3,2,0:T(8,128)(2,1)} fusion(f32[64,2,64,64]{3,2,1,0:T(8,128)} %fusion.8, bf16[64,64,2,64]{1,0,3,2:T(8,128)(2,1)} %reshape_reshape.9, f32[64,64,2]{1,2,0:T(2,128)S(1)} %copy.137, f32[64,2,64]{2,1,0:T(2,128)S(1)} %copy.123, f32[64,2,64]{2,1,0:T(2,128)S(1)} %copy.121, pred[64,64]{1,0:T(8,128)(4,1)S(1)} %iota_compare_fusion.1, ...), kind=kOutput, calls=%fused_computation.16 | convolution fusion | flops 206045184 | bytes 8491008 | tf_op jit(solution)/shard_map/bhts,bshp->bthp/dot_general | solution.py:56
  310.9 4.3 %copy.138 = bf16[64,64,2,64]{1,0,3,2:T(8,128)(2,1)} copy(bf16[64,64,2,64]{1,3,2,0:T(8,128)(2,1)} %fusion.7) | data formatting | bytes 2097152 | tf_op jit(solution)/shard_map/convert_element_type | solution.py:150
  315.2 3.2 convert_element_type.123
  318.7 36.4 %all_to_all.80 = bf16[8,512,128]{1,2,0:T(8,128)(2,1)S(1)} all-to-all(bf16[8,512,128]{1,2,0:T(8,128)(2,1)S(1)} %copy.139), channel_id=1, replica_groups=mesh['sp'=8,'dp'=4] {'sp'}, dimensions={0} | all-to-all | bytes 2097152 | tf_op jit(solution)/shard_map/all_to_all | solution.py:151
  355.1 1.6 convert_element_type.134
  356.7 2.9 copy.142
  359.6 6.9 %multiply_reduce_fusion = (f32[512]{0:T(512)S(1)}, f32[512,1024]{1,0:T(8,128)}) fusion(f32[512,1024]{1,0:T(8,128)} %copy.142, bf16[2048,1024]{1,0:T(8,128)(2,1)} %all-gather.12.cloned.1.call-done, bf16[1,512,2048]{2,1,0:T(8,128)(2,1)S(1)} %copy-done), kind=kOutput, calls=%fused_computation.57 | convolution fusion | flops 2152201728 | bytes 10487808 | tf_op jit(solution)/shard_map/dot_general | solution.py:103
  366.6 9.2 %all-gather.14.cloned.1.call-done = bf16[1024,2048]{0,1:T(8,128)(2,1)} async-done(((bf16[1024,64]{0,1:T(8,128)(2,1)}), bf16[1024,2048]{0,1:T(8,128)(2,1)}) %all-gather.14.cloned.1.call-update) | async-done | bytes 4194320 | tf_op jit(solution)/shard_map/all_gather | solution.py:157
  375.8 6.5 %fusion.12 = bf16[1,512,2048]{2,1,0:T(8,128)(2,1)} fusion(bf16[1024,2048]{0,1:T(8,128)(2,1)} %all-gather.14.cloned.1.call-done, f32[512,1024]{1,0:T(8,128)} %get-tuple-element.20, f32[1024]{0:T(1024)S(1)} %copy-done.6, f32[512]{0:T(512)S(1)} %add_rsqrt_fusion), kind=kOutput, calls=%fused_computation.27 | convolution fusion | flops 2150105088 | bytes 8394752 | tf_op jit(solution)/shard_map/dot_general | solution.py:155
  (62 shorter events, 5.7 us)
Async XLA Ops:
  6.5 2.8 copy-start
  6.5 60.1 %all-gather.10.cloned.1.call-start = ((), (), s32[]{:S(2)}) async-start(), calls=%async_computation.7 | async-start | bytes 2162688 | tf_op jit(solution)/shard_map/all_gather | solution.py:111
  7.3 141.2 %all-gather.8.cloned.1.call-start = ((), (), s32[]{:S(2)}) async-start(), calls=%async_computation.6 | async-start | bytes 2162688 | tf_op jit(solution)/shard_map/all_gather | solution.py:112
  8.0 229.1 %all-gather.6.cloned.1.call-start = ((), (), s32[]{:S(2)}) async-start(), calls=%async_computation.5 | async-start | bytes 4325376 | tf_op jit(solution)/shard_map/all_gather | solution.py:109
  8.7 350.9 %all-gather.12.cloned.1.call-start = ((), (), s32[]{:S(2)}) async-start(), calls=%async_computation.8 | async-start | bytes 4325376 | tf_op jit(solution)/shard_map/all_gather | solution.py:110
  11.4 58.1 %all-to-all-start.3 = ((bf16[512,8,2]{0,2,1:T(2,128)(2,1)}), bf16[512,8,2]{0,2,1:T(2,128)(2,1)S(1)}, u32[]{:S(2)}, u32[]{:S(2)}) async-start(bf16[512,8,2]{0,2,1:T(2,128)(2,1)} %all_to_all.72), calls=%async_computation.3 | async-start | bytes 32768 | tf_op jit(solution)/shard_map/all_to_all | solution.py:124
  71.1 80.3 %all-to-all-start.2 = ((bf16[512,8,256]{0,2,1:T(8,128)(2,1)}), bf16[512,8,256]{0,2,1:T(8,128)(2,1)}, u32[]{:S(2)}, u32[]{:S(2)}) async-start(bf16[512,8,256]{0,2,1:T(8,128)(2,1)} %bitcast.114), calls=%async_computation.2 | async-start | bytes 4194304 | tf_op jit(solution)/shard_map/all_to_all | solution.py:122
  76.7 299.1 %all-gather.14.cloned.1.call-start = ((), (), s32[]{:S(2)}) async-start(), calls=%async_computation.9 | async-start | bytes 4325376 | tf_op jit(solution)/shard_map/all_gather | solution.py:157
  152.9 6.0 %copy-start.7 = (f32[16]{0:T(128)S(1)}, f32[16]{0:T(128)}, u32[]{:S(2)}) copy-start(f32[16]{0:T(128)} %param.23) | copy-start | bytes 196
  152.9 6.1 %copy-start.8 = (f32[16]{0:T(128)S(1)}, f32[16]{0:T(128)}, u32[]{:S(2)}) copy-start(f32[16]{0:T(128)} %param.22) | copy-start | bytes 196
  152.9 6.2 %copy-start.4 = (bf16[4,512]{1,0:T(4,128)(2,1)S(1)}, bf16[4,512]{1,0:T(4,128)(2,1)}, u32[]{:S(2)}) copy-start(bf16[4,512]{1,0:T(4,128)(2,1)} %param.21) | copy-start | bytes 12292
  152.9 6.2 %copy-start.5 = (bf16[4,512]{1,0:T(4,128)(2,1)S(1)}, bf16[4,512]{1,0:T(4,128)(2,1)}, u32[]{:S(2)}) copy-start(bf16[4,512]{1,0:T(4,128)(2,1)} %param.20) | copy-start | bytes 12292
  152.9 60.8 %all-to-all-start.1 = ((bf16[512,8,256]{0,2,1:T(8,128)(2,1)}), bf16[512,8,256]{0,2,1:T(8,128)(2,1)}, u32[]{:S(2)}, u32[]{:S(2)}) async-start(bf16[512,8,256]{0,2,1:T(8,128)(2,1)} %bitcast.113), calls=%async_computation.1 | async-start | bytes 4194304 | tf_op jit(solution)/shard_map/all_to_all | solution.py:123
  164.2 1.3 copy-start.1
  168.2 3.3 slice-start
  242.9 33.4 %all-to-all-start = ((bf16[512,8,128]{2,0,1:T(8,128)(2,1)}), bf16[512,8,128]{2,0,1:T(8,128)(2,1)S(1)}, u32[]{:S(2)}, u32[]{:S(2)}) async-start(bf16[512,8,128]{2,0,1:T(8,128)(2,1)} %bitcast.119), calls=%async_computation | async-start | bytes 2097152 | tf_op jit(solution)/shard_map/all_to_all | solution.py:119
  283.4 2.4 copy-start.3
  288.4 6.7 %copy-start.2 = (bf16[64,64,2,128]{3,2,1,0:T(2,128)(2,1)S(1)}, bf16[64,64,2,128]{3,2,1,0:T(2,128)(2,1)}, u32[]{:S(2)}) copy-start(bf16[64,64,2,128]{3,2,1,0:T(2,128)(2,1)} %reshape_reshape.10) | copy-start | bytes 6291460
  359.6 16.2 %copy-start.6 = (f32[1024]{0:T(1024)S(1)}, f32[1024]{0:T(1024)}, u32[]{:S(2)}) copy-start(f32[1024]{0:T(1024)} %param.24) | copy-start | bytes 12292
Sparse Core Ops, SparseCore 0:
  10.2 56.3 all-gather.9
  69.5 78.9 all-gather.7
  151.3 85.7 all-gather.5
  239.9 68.4 all-gather.11
  311.1 64.6 all-gather.13
where the time goes:
time: 396 us; the launch traced here: 389 us
  waiting for transfers between devices  193 us (49%)
  local copies, waits for them, and re-layouts  53.9 us (14%)
  matrix products  50.3 us (13%)
  blocking collectives  36.4 us (9%)
  starting transfers between devices  22.4 us (6%)
  other arithmetic  19.1 us (5%)
  between operations  13.6 us (3%)
    all_gather x1, waiting for transfers between devices, per_device(): lax.all_gather(readout_weight, ('sp', 'dp'), axis=0, tiled=True)  70.5 us
    all_gather x1, waiting for transfers between devices, per_device(): lax.all_gather(input_weight, ('sp', 'dp'), axis=0, tiled=True)  49.7 us
    all_to_all x1, blocking collectives, per_device(): lax.all_to_all(mixed, 'sp', split_axis=0, concat_axis=1, tiled=True)  36.4 us
    all_to_all x1, waiting for transfers between devices, per_device(): lax.all_to_all(wide_reads, 'sp', split_axis=1, concat_axis=0, tiled=True)  22.7 us
    all_gather x1, waiting for transfers between devices, per_device(): lax.all_gather(value_weight, ('sp', 'dp'), axis=0, tiled=True)  19.5 us
    all_to_all x1, waiting for transfers between devices, per_device(): lax.all_to_all(value_sum.astype(jnp.bfloat16), 'sp', split_axis=1, concat...  18.6 us
    dot_general x4, matrix products, add_rows(): return jnp.dot(sequence, piece, preferred_element_type=jnp.float32)  17.2 us
    all_gather x1, waiting for transfers between devices, per_device(): lax.all_gather(out_weight, ('sp', 'dp'), axis=1, tiled=True)  9.22 us
  transfers between devices with their start and end apart: 9, of which 6 were waited for; matrix products, arithmetic and copies ran while one was open for 30% of the time, Pallas kernels for 0%

commit v1 on v0

v1 whole, which is shorter than its diff:
```python
import functools

import jax
import jax.numpy as jnp
from jax import lax
from jax.experimental import pallas as pl
from jax.experimental.pallas import tpu as pltpu
from jax.sharding import PartitionSpec as P

GROUPS = 4
CHUNK = 128
HALO = 16
norm_eps = 1.0
F32 = jnp.float32
BF16 = jnp.bfloat16


def conv_silu(ref, start, taps_ref, col, width):
    x = ref[pl.ds(start, CHUNK + HALO), col : col + width].astype(F32)
    extent = taps_ref.shape[0]
    total = None
    for k in range(extent):
        shift = extent - 1 - k
        moved = pltpu.roll(x, shift, 0) if shift else x
        term = taps_ref[k : k + 1, col : col + width].astype(F32) * moved[HALO:]
        total = term if total is None else total + term
    return (total / (1.0 + jnp.exp(-total))).astype(BF16)


def states_kernel(
    v_ref, b_ref, vt_ref, bt_ref, tail_ref, cdec_ref, cv_ref, cb_ref, cr_ref, prefix_ref, final_ref
):
    c = pl.program_id(0)
    start = c * CHUNK
    state = cb_ref.shape[1] // GROUPS
    wide = cv_ref.shape[1] // GROUPS

    @pl.when(c == 0)
    def _():
        final_ref[...] = jnp.zeros(final_ref.shape, F32)

    for g in range(GROUPS):
        values = conv_silu(v_ref, start, vt_ref, g * wide, wide)
        cv_ref[:, g * wide : (g + 1) * wide] = values
        inputs = conv_silu(b_ref, start, bt_ref, g * state, state)
        cb_ref[:, g * state : (g + 1) * state] = inputs
        reads = conv_silu(b_ref, start, bt_ref, (GROUPS + g) * state, state)
        cr_ref[:, g * state : (g + 1) * state] = reads
        weighted = (values.astype(F32) * tail_ref[:, g * wide : (g + 1) * wide]).astype(BF16)
        added = lax.dot_general(inputs, weighted, (((0,), (0,)), ((), ())), preferred_element_type=F32)
        rows = slice(g * state, (g + 1) * state)
        old = final_ref[rows, :]
        prefix_ref[0, rows, :] = old.astype(BF16)
        keep = cdec_ref[pl.ds(c, 1), g * wide : (g + 1) * wide]
        final_ref[rows, :] = old * keep + added


def within_kernel(cv_ref, cb_ref, cr_ref, prefix_ref, cum_ref, cumt_ref, ratet_ref, erun_ref, out_ref):
    state = cb_ref.shape[1] // GROUPS
    wide = cv_ref.shape[1] // GROUPS
    heads = cum_ref.shape[1]
    width = cv_ref.shape[1] // heads
    per_group = heads // GROUPS
    t = lax.broadcasted_iota(jnp.int32, (CHUNK, CHUNK), 0)
    s = lax.broadcasted_iota(jnp.int32, (CHUNK, CHUNK), 1)
    causal = s <= t
    low = lax.broadcasted_iota(jnp.int32, (CHUNK, 2 * width), 1) < width
    zero = jnp.zeros((CHUNK, 2 * width), BF16)
    for g in range(GROUPS):
        reads = cr_ref[:, g * state : (g + 1) * state]
        inputs = cb_ref[:, g * state : (g + 1) * state]
        inter = lax.dot_general(reads, inputs, (((1,), (1,)), ((), ())), preferred_element_type=F32)
        across = jnp.dot(reads, prefix_ref[0, g * state : (g + 1) * state, :], preferred_element_type=F32)
        for pair in range(per_group // 2):
            scores = []
            for j in range(2):
                h = g * per_group + 2 * pair + j
                gap = jnp.minimum(cum_ref[:, h : h + 1] - cumt_ref[h : h + 1, :], 0.0)
                sc = inter * jnp.exp(gap) * ratet_ref[h : h + 1, :]
                scores.append(jnp.where(causal, sc, 0.0).astype(BF16))
            col = g * wide + pair * 2 * width
            vals = cv_ref[:, col : col + 2 * width]
            split = jnp.concatenate([jnp.where(low, vals, zero), jnp.where(low, zero, vals)], axis=0)
            inside = jnp.dot(jnp.concatenate(scores, axis=1), split, preferred_element_type=F32)
            part = across[:, pair * 2 * width : (pair + 1) * 2 * width]
            out_ref[:, col : col + 2 * width] = inside + part * erun_ref[:, col : col + 2 * width]


def finish_kernel(part_ref, cr_ref, enter_ref, ecum_ref, *rest):
    gate_refs, (gain_ref, out_ref) = rest[:-2], rest[-2:]
    state = cr_ref.shape[1] // GROUPS
    wide = part_ref.shape[1] // GROUPS
    pieces = []
    for g in range(GROUPS):
        reads = cr_ref[:, g * state : (g + 1) * state]
        far = jnp.dot(reads, enter_ref[g * state : (g + 1) * state, :], preferred_element_type=F32)
        cols = slice(g * wide, (g + 1) * wide)
        pieces.append((part_ref[:, cols] + far * ecum_ref[:, cols]).astype(BF16).astype(F32))
    mixed = jnp.concatenate(pieces, axis=1)
    gate = jnp.concatenate([r[...] for r in gate_refs], axis=1).astype(F32)
    gated = mixed * (gate / (1.0 + jnp.exp(-gate)))
    scale = lax.rsqrt(jnp.mean(gated * gated, axis=-1, keepdims=True) + norm_eps)
    out_ref[...] = (gated * scale * gain_ref[...]).astype(BF16)


def whole(shape):
    return pl.BlockSpec(shape, lambda c: (0,) * len(shape))


def rows(width):
    return pl.BlockSpec((CHUNK, width), lambda c: (c, 0))


def shift_before(x, axis, size, distance):
    return lax.ppermute(x, axis, [(i, i + distance) for i in range(size - distance)])


def sequence_part(values, mix, gates, taps, rate_raw, rate_bias, decay_log, norm_gain, length, sp, index):
    value_taps, mix_taps = taps
    local = values.shape[0] - HALO
    chunks = local // CHUNK
    width = values.shape[1]
    heads = rate_bias.shape[0]
    wide = width // GROUPS
    keys = mix.shape[1] // 2
    state = keys // GROUPS
    spread = functools.partial(jnp.repeat, repeats=width // heads, axis=1)
    rate = jax.nn.softplus(rate_raw.astype(F32) + rate_bias)
    decay = -jnp.exp(decay_log) / length
    tri = jnp.tril(jnp.ones((local, local), F32))
    cum = jnp.dot(tri, rate * decay, precision=lax.Precision.HIGHEST)
    ends = cum[CHUNK - 1 :: CHUNK]
    starts = jnp.concatenate([jnp.zeros((1, heads), F32), ends[:-1]], axis=0)
    end_rows = jnp.repeat(ends, CHUNK, axis=0)
    start_rows = jnp.repeat(starts, CHUNK, axis=0)
    tail = spread(jnp.exp(jnp.minimum(end_rows - cum, 0.0)) * rate)
    erun = spread(jnp.exp(jnp.minimum(cum - start_rows, 0.0)))
    ecum = spread(jnp.exp(cum))
    cdec = spread(jnp.exp(ends - starts))
    cumt = cum.T
    ratet = rate.T
    totals = lax.all_gather(cum[-1], "sp")
    tail, erun, ecum, cdec, cumt, ratet, totals = lax.optimization_barrier(
        (tail, erun, ecum, cdec, cumt, ratet, totals)
    )
    arb = pltpu.CompilerParams(dimension_semantics=("arbitrary",))
    cv, cb, cr, prefix, final = pl.pallas_call(
        states_kernel,
        grid=(chunks,),
        in_specs=[
            whole(values.shape),
            whole(mix.shape),
            whole(value_taps.shape),
            whole(mix_taps.shape),
            rows(width),
            whole(cdec.shape),
        ],
        out_specs=[
            rows(width),
            rows(keys),
            rows(keys),
            pl.BlockSpec((1, keys, wide), lambda c: (c, 0, 0)),
            whole((keys, wide)),
        ],
        out_shape=[
            jax.ShapeDtypeStruct((local, width), BF16),
            jax.ShapeDtypeStruct((local, keys), BF16),
            jax.ShapeDtypeStruct((local, keys), BF16),
            jax.ShapeDtypeStruct((chunks, keys, wide), BF16),
            jax.ShapeDtypeStruct((keys, wide), F32),
        ],
        compiler_params=arb,
        name="states",
    )(values, mix, value_taps, mix_taps, tail, cdec)
    device = lax.broadcasted_iota(jnp.int32, (sp, 1), 0)
    own = spread(jnp.exp(cum[-1:]))

    def by_head(row):
        return jnp.repeat(row.reshape(GROUPS, 1, wide), state, axis=1).reshape(keys, wide)

    own = by_head(own)
    entering = None
    window = 0
    while window < sp - 1:
        inclusive = final if entering is None else final + own * entering
        got = shift_before(inclusive.astype(BF16), "sp", sp, window + 1).astype(F32)
        if entering is None:
            entering = got
        else:
            near = (device >= index - window) & (device < index)
            span = jnp.sum(jnp.where(near, totals, 0.0), axis=0, keepdims=True)
            entering = entering + by_head(spread(jnp.exp(span))) * got
        window = 2 * window + 1
    entering = entering.astype(BF16) if entering is not None else jnp.zeros((keys, wide), BF16)
    part = pl.pallas_call(
        within_kernel,
        grid=(chunks,),
        in_specs=[
            rows(width),
            rows(keys),
            rows(keys),
            pl.BlockSpec((1, keys, wide), lambda c: (c, 0, 0)),
            rows(heads),
            pl.BlockSpec((heads, CHUNK), lambda c: (0, c)),
            pl.BlockSpec((heads, CHUNK), lambda c: (0, c)),
            rows(width),
        ],
        out_specs=rows(width),
        out_shape=jax.ShapeDtypeStruct((local, width), F32),
        compiler_params=arb,
        name="within",
    )(cv, cb, cr, prefix, cum, cumt, ratet, erun)
    return pl.pallas_call(
        finish_kernel,
        grid=(chunks,),
        in_specs=[rows(width), rows(keys), whole((keys, wide)), rows(width)]
        + [rows(g.shape[1]) for g in gates]
        + [whole((1, width))],
        out_specs=rows(width),
        out_shape=jax.ShapeDtypeStruct((local, width), BF16),
        compiler_params=arb,
        name="finish",
    )(part, cr, entering, ecum, *gates, norm_gain.reshape(1, width))


def make_per_device(mesh):
    sp = mesh.shape["sp"]

    def per_device(
        activations,
        value_weight,
        gate_weight,
        input_weight,
        readout_weight,
        rate_weight,
        value_taps,
        input_taps,
        readout_taps,
        rate_bias,
        decay_log,
        norm_gain,
        out_weight,
    ):
        own = activations[0]
        index = lax.axis_index("sp")
        halo = shift_before(own[-HALO:], "sp", sp, 1)
        joined = jnp.concatenate([value_weight, input_weight, readout_weight, gate_weight], axis=1)
        weights = lax.all_gather(joined, ("sp", "dp"), axis=0, tiled=True)
        out_rows = lax.all_gather(out_weight.T, ("sp", "dp"), axis=0, tiled=True)
        sequence = jnp.concatenate([halo, own], axis=0)
        rate_raw = jnp.dot(own, rate_weight, preferred_element_type=F32).astype(BF16)
        width = value_weight.shape[1]
        keys = input_weight.shape[1]
        values = jnp.dot(sequence, weights[:, :width], preferred_element_type=F32).astype(BF16)
        mix = jnp.dot(
            sequence, weights[:, width : width + 2 * keys], preferred_element_type=F32
        ).astype(BF16)
        gate = jnp.dot(own, weights[:, width + 2 * keys :], preferred_element_type=F32).astype(BF16)
        taps = (value_taps, jnp.concatenate([input_taps, readout_taps], axis=1))
        normed = sequence_part(
            values, mix, (gate,), taps, rate_raw, rate_bias, decay_log, norm_gain,
            own.shape[0] * sp, sp, index,
        )
        result = lax.dot_general(
            normed, out_rows, (((1,), (1,)), ((), ())), preferred_element_type=F32
        )
        return result.astype(BF16)[None]

    return per_device


def solution(mesh):
    rows_split = P(("sp", "dp"), None)
    placed = (P("dp", "sp", None),) + (rows_split,) * 4 + (P(),) * 7 + (P(None, ("sp", "dp")),)
    return jax.shard_map(
        make_per_device(mesh),
        mesh=mesh,
        in_specs=placed,
        out_specs=P("dp", "sp", None),
        check_vma=False,
    )
```

time: 396 us -> 196 us (0.49); the launches traced: 389 us -> 195 us
  waiting for transfers between devices: 193 us -> 93.9 us
  local copies, waits for them, and re-layouts: 53.9 us -> 14.8 us
  blocking collectives: 36.4 us -> 11.4 us
  matrix products: 50.3 us -> 28.4 us
  Pallas kernels: 0 us -> 18.2 us
  starting transfers between devices: 22.4 us -> 8.12 us
  other arithmetic: 19.1 us -> 6.49 us
    all_gather x5 -> x2, waiting for transfers between devices: 149 us -> 68.2 us  [the longest x1 68.2 us: per_device(): weights = lax.all_gather(joined, ('sp', 'dp'), axis=0, tiled=True)]
    all_to_all x4 -> x0, waiting for transfers between devices: 41.3 us -> none  [the longest x1 22.7 us: per_device(): lax.all_to_all(wide_reads, 'sp', split_axis=1, concat_axis=0, tiled=True)]
    all_to_all x1 -> x0, blocking collectives: 36.4 us -> none  [per_device(): lax.all_to_all(mixed, 'sp', split_axis=0, concat_axis=1, tiled=True)]
    ppermute x0 -> x4, waiting for transfers between devices: none -> 25 us  [shift_before(): lax.ppermute(x, axis, [(i, i + distance) for i in range(size - distance)])]
    all_to_all x4 -> x0, starting transfers between devices: 22.3 us -> none  [the longest x1 6 us: per_device(): lax.all_to_all(wide_reads, 'sp', split_axis=1, concat_axis=0, tiled=True)]
    dot_general x10 -> x6, matrix products: 50.3 us -> 28.4 us  [the longest x1 6.71 us: per_device(): jnp.dot(own, weights[:, width + 2 * keys:], preferred_element_type=F32)]
    pallas_call x0 -> x3, Pallas kernels: none -> 18.2 us  [the longest x1 6.64 us: sequence_part(): pl.pallas_call(states_kernel, grid=(chunks,), in_specs=[whole(values.shap...]
    another operation x5 -> x0, local copies, waits for them, and re-layouts: 14.9 us -> none  [the longest x1 4.23 us: block_parts(): block_values = values.reshape(blocks, BLOCK, head_count, head_width)]
  transfers between devices with their start and end apart: 9 -> 6, of which waited for: 6 -> 4; matrix products, arithmetic and copies ran while one was open for 30% -> 21% of each run, Pallas kernels for 0% -> 9%
where the time goes in v1:
time: 196 us; the launch traced here: 195 us
  waiting for transfers between devices  93.9 us (48%)
  matrix products  28.4 us (14%)
  Pallas kernels  18.2 us (9%)
  local copies, waits for them, and re-layouts  14.8 us (8%)
  between operations  13.5 us (7%)
  blocking collectives  11.4 us (6%)
  starting transfers between devices  8.12 us (4%)
  other arithmetic  6.49 us (3%)
    all_gather x1, waiting for transfers between devices, per_device(): weights = lax.all_gather(joined, ('sp', 'dp'), axis=0, tiled=True)  68.2 us
    ppermute x4, waiting for transfers between devices, shift_before(): lax.ppermute(x, axis, [(i, i + distance) for i in range(size - distance)])  25 us
    all_gather x1, blocking collectives, sequence_part(): totals = lax.all_gather(cum[-1], 'sp')  11.4 us
    ppermute x4, starting transfers between devices, shift_before(): lax.ppermute(x, axis, [(i, i + distance) for i in range(size - distance)])  8.07 us
    optimization_barrier x3, local copies, waits for them, and re-layouts, sequence_part(): lax.optimization_barrier((tail, erun, ecum, cdec, cumt, ratet, totals))  7.67 us
    dot_general x1, matrix products, per_device(): jnp.dot(own, weights[:, width + 2 * keys:], preferred_element_type=F32)  6.71 us
    pallas_call x1, Pallas kernels, sequence_part(): pl.pallas_call(states_kernel, grid=(chunks,), in_specs=[whole(values.shap...  6.64 us
    pallas_call x1, Pallas kernels, sequence_part(): pl.pallas_call(within_kernel, grid=(chunks,), in_specs=[rows(width), rows...  6.4 us
  transfers between devices with their start and end apart: 6, of which 4 were waited for; matrix products, arithmetic and copies ran while one was open for 21% of the time, Pallas kernels for 9%

profile of v1, /device:TPU:29, one launch (start us, length us, event | category | flops | bytes accessed | tf_op | source)
XLA Modules:
  0.0 194.8 jit_solution(8913429298283689327)
XLA Ops:
  6.5 1.8 pad_maximum_fusion.3
  8.5 0.7 all-gather.6.cloned.1.call-update
  9.2 0.8 slice_bitcast_fusion
  10.0 3.1 %collective-permute-start = (bf16[16,2048]{1,0:T(8,128)(2,1)S(1)}, bf16[16,2048]{1,0:T(8,128)(2,1)S(1)}, u32[]{:S(2)}, u32[]{:S(2)}) collective-permute-start(bf16[16,2048]{1,0:T(8,128)(2,1)S(1)} %slice_bitcast_fusion), channel_id=1, source_target_pairs={{0,4},{4,8},{8,12},{12,16},{16,20},{20,24},{24,28},{1,5},{5,9},{9,... | collective-permute-start | bytes 196616 | tf_op jit(solution)/shard_map/ppermute | solution.py:115
  13.1 0.7 negate_multiply_fusion
  13.8 2.9 %compare_select_fusion = (f32[16,512]{1,0:T(8,128)}, f32[512,16]{0,1:T(8,128)S(1)}) fusion(f32[16]{0:T(128)} %param.22, bf16[2048,16]{0,1:T(8,128)(2,1)S(1)} %copy-done, bf16[1,512,2048]{2,1,0:T(8,128)(2,1)} %param.13), kind=kOutput, calls=%fused_computation.33 | convolution fusion | flops 33628160 | bytes 2228288 | tf_op jit(solution)/shard_map/dot_general | solution.py:251
  16.7 0.7 fusion.21
  17.4 0.1 slice.29
  17.4 0.1 subtract_exponential_fusion
  17.5 0.1 copy.24
  17.6 0.1 broadcast_in_dim.83
  17.7 0.7 reshape.74.cdec_ref
  18.4 0.2 exponential_reduce_fusion
  18.6 11.4 %all-gather = f32[8,1,16]{2,1,0:T(1,128)S(1)} all-gather(f32[1,1,16]{2,1,0:T(1,128)S(1)} %bitcast.98), channel_id=1, replica_groups=mesh['sp'=8,'dp'=4] {'sp'}, dimensions={0}, use_global_device_ids=true | all-gather | bytes 576 | tf_op jit(solution)/shard_map/all_gather | solution.py:142
  30.1 0.1 broadcast_in_dim.80
  30.2 0.3 broadcast_in_dim.82
  30.5 1.6 broadcast_in_dim.81
  32.1 1.6 broadcast_in_dim.79
  33.7 2.9 %copy.25.tail_ref = f32[512,1024]{1,0:T(8,128)} copy(f32[512,1024]{0,1:T(8,128)} %bitcast.88) | data formatting | bytes 4194304 | tf_op jit(solution)/shard_map/optimization_barrier | solution.py:143
  36.6 0.6 pad_maximum_fusion.4.bt_ref
  37.2 68.2 %all-gather.4.cloned.1.call-done = bf16[2048,3072]{1,0:T(8,128)(2,1)} async-done(((bf16[64,3072]{1,0:T(8,128)(2,1)}), bf16[2048,3072]{1,0:T(8,128)(2,1)}) %all-gather.4.cloned.1.call-update) | async-done | bytes 12582928 | tf_op jit(solution)/shard_map/all_gather | solution.py:248
  105.4 6.3 %fusion.10.b_ref = bf16[528,1024]{1,0:T(8,128)(2,1)} fusion(bf16[2048,3072]{1,0:T(8,128)(2,1)} %all-gather.4.cloned.1.call-done, bf16[512,2048]{1,0:T(8,128)(2,1)} %bitcast.89, bf16[16,2048]{1,0:T(8,128)(2,1)S(1)} %collective-permute-done), kind=kOutput, calls=%fused_computation.10 | convolution fusion | flops 2219458560 | bytes 7438336 | tf_op jit(solution)/shard_map/dot_general | solution.py:255
  111.8 5.6 %fusion.7.v_ref = bf16[528,1024]{1,0:T(8,128)(2,1)} fusion(bf16[2048,3072]{1,0:T(8,128)(2,1)} %all-gather.4.cloned.1.call-done, bf16[512,2048]{1,0:T(8,128)(2,1)S(1)} %bitcast.90, bf16[16,2048]{1,0:T(8,128)(2,1)S(1)} %collective-permute-done), kind=kOutput, calls=%fused_computation.9 | convolution fusion | flops 2219458560 | bytes 7438336 | tf_op jit(solution)/shard_map/dot_general | solution.py:254
  117.3 6.6 %states.1 = (bf16[512,1024]{1,0:T(8,128)(2,1)}, bf16[512,512]{1,0:T(8,128)(2,1)}, bf16[512,512]{1,0:T(8,128)(2,1)}, bf16[4,512,256]{2,1,0:T(8,128)(2,1)}, f32[512,256]{1,0:T(8,128)}) custom-call(bf16[528,1024]{1,0:T(8,128)(2,1)} %fusion.7.v_ref, bf16[528,1024]{1,0:T(8,128)(2,1)} %fusion.10.b_ref, bf16[4,1024]{1,0:T(4,128)(2,1)} %vt_ref.1, ...), custom_call_target="tpu_custom_call" | custom-call | tf_op jit(solution)/shard_map/states/pallas_call | solution.py:147
  124.0 1.1 convert_element_type.49
  125.0 2.2 %collective-permute-start.1 = (bf16[512,256]{1,0:T(8,128)(2,1)S(1)}, bf16[512,256]{1,0:T(8,128)(2,1)S(1)}, u32[]{:S(2)}, u32[]{:S(2)}) collective-permute-start(bf16[512,256]{1,0:T(8,128)(2,1)S(1)} %convert_element_type.49), channel_id=1, source_target_pairs={{0,4},{4,8},{8,12},{12,16},{16,20},{20,24},{24,28},{1,5},{5,9},{9,... | collective-permute-start | bytes 786440 | tf_op jit(solution)/shard_map/ppermute | solution.py:115
  127.2 0.1 broadcast_in_dim.89
  127.4 0.1 broadcast_in_dim.91
  127.5 8.1 %collective-permute-done.1 = bf16[512,256]{1,0:T(8,128)(2,1)S(1)} collective-permute-done((bf16[512,256]{1,0:T(8,128)(2,1)S(1)}, bf16[512,256]{1,0:T(8,128)(2,1)S(1)}, u32[]{:S(2)}, u32[]{:S(2)}) %collective-permute-start.1) | collective-permute-done | bytes 262176 | tf_op jit(solution)/shard_map/ppermute | solution.py:115
  135.6 1.1 fusion.24
  136.7 1.3 collective-permute-start.2
  138.0 0.8 copy.26.cum_ref
  138.9 0.1 select_reduce_fusion
  139.0 0.1 exp.53
  139.0 0.1 exp.56
  139.2 0.1 broadcast_in_dim.95
  139.4 0.1 broadcast_in_dim.87
  139.4 2.9 %copy.27.erun_ref = f32[512,1024]{1,0:T(8,128)} copy(f32[512,1024]{0,1:T(8,128)} %bitcast.87) | data formatting | bytes 4194304 | tf_op jit(solution)/shard_map/optimization_barrier | solution.py:143
  142.3 1.8 copy.29.ecum_ref
  144.2 5.4 %collective-permute-done.2 = bf16[512,256]{1,0:T(8,128)(2,1)S(1)} collective-permute-done((bf16[512,256]{1,0:T(8,128)(2,1)S(1)}, bf16[512,256]{1,0:T(8,128)(2,1)S(1)}, u32[]{:S(2)}, u32[]{:S(2)}) %collective-permute-start.2) | collective-permute-done | bytes 262176 | tf_op jit(solution)/shard_map/ppermute | solution.py:115
  149.5 0.1 fusion.26
  149.7 1.5 collective-permute-start.3
  151.2 6.7 %fusion.16.rest_0_ = bf16[512,1024]{1,0:T(8,128)(2,1)} fusion(bf16[2048,3072]{1,0:T(8,128)(2,1)} %all-gather.4.cloned.1.call-done, bf16[1,512,2048]{2,1,0:T(8,128)(2,1)} %param.13), kind=kOutput, calls=%fused_computation.12 | convolution fusion | flops 2148007936 | bytes 7340032 | tf_op jit(solution)/shard_map/dot_general | solution.py:258
  157.9 6.4 %within.1.part_ref = f32[512,1024]{1,0:T(8,128)} custom-call(bf16[512,1024]{1,0:T(8,128)(2,1)} %get-tuple-element.19.cv_ref, bf16[512,512]{1,0:T(8,128)(2,1)} %get-tuple-element.20.cb_ref, bf16[512,512]{1,0:T(8,128)(2,1)} %get-tuple-element.21.cr_ref, bf16[4,512,256]{2,1,0:T(8,128)(2,1)} %get-tuple-element.22.prefix_ref, f32[512,16]{1,0:T(8,128)} %copy.26.cum_ref, ...), custom_call_target="tpu_custom_call" | custom-call | tf_op jit(solution)/shard_map/within/pallas_call | solution.py:195
  164.3 11.5 %collective-permute-done.3 = bf16[512,256]{1,0:T(8,128)(2,1)S(1)} collective-permute-done((bf16[512,256]{1,0:T(8,128)(2,1)S(1)}, bf16[512,256]{1,0:T(8,128)(2,1)S(1)}, u32[]{:S(2)}, u32[]{:S(2)}) %collective-permute-start.3) | collective-permute-done | bytes 262176 | tf_op jit(solution)/shard_map/ppermute | solution.py:115
  175.8 0.8 fusion.28.enter_ref
  176.6 5.2 %finish.1 = bf16[512,1024]{1,0:T(8,128)(2,1)} custom-call(f32[512,1024]{1,0:T(8,128)} %within.1.part_ref, bf16[512,512]{1,0:T(8,128)(2,1)} %get-tuple-element.21.cr_ref, bf16[512,256]{1,0:T(8,128)(2,1)} %fusion.28.enter_ref, f32[512,1024]{1,0:T(8,128)} %copy.29.ecum_ref, bf16[512,1024]{1,0:T(8,128)(2,1)} %fusion.16.rest_0_, f32[1,1024]{1,0:T(1,128)} %bitcast.97), custom_call_target="tpu_custom_call" | custom-call | tf_op jit(solution)/shard_map/finish/pallas_call | solution.py:213
  181.8 6.2 %fusion.6 = bf16[1,512,2048]{2,1,0:T(8,128)(2,1)} fusion(bf16[512,1024]{1,0:T(8,128)(2,1)} %finish.1, bf16[2048,1024]{1,0:T(8,128)(2,1)} %all-gather.6.cloned.1.call-done), kind=kOutput, calls=%fused_computation.7 | convolution fusion | flops 2148532224 | bytes 7340032 | tf_op jit(solution)/shard_map/dot_general | solution.py:264
  (25 shorter events, 0.5 us)
Async XLA Ops:
  6.5 7.2 %copy-start = (bf16[2048,16]{0,1:T(8,128)(2,1)S(1)}, bf16[2048,16]{0,1:T(8,128)(2,1)}, u32[]{:S(2)}) copy-start(bf16[2048,16]{0,1:T(8,128)(2,1)} %param.18) | copy-start | bytes 196612
  6.5 98.9 %all-gather.4.cloned.1.call-start = ((), (), s32[]{:S(2)}) async-start(), calls=%async_computation | async-start | bytes 12976128 | tf_op jit(solution)/shard_map/all_gather | solution.py:248
  8.4 173.4 %all-gather.6.cloned.1.call-start = ((), (), s32[]{:S(2)}) async-start(), calls=%async_computation.1 | async-start | bytes 4325376 | tf_op jit(solution)/shard_map/all_gather | solution.py:249
  10.0 27.2 %collective-permute-start = (bf16[16,2048]{1,0:T(8,128)(2,1)S(1)}, bf16[16,2048]{1,0:T(8,128)(2,1)S(1)}, u32[]{:S(2)}, u32[]{:S(2)}) collective-permute-start(bf16[16,2048]{1,0:T(8,128)(2,1)S(1)} %slice_bitcast_fusion), channel_id=1, source_target_pairs={{0,4},{4,8},{8,12},{12,16},{16,20},{20,24},{24,28},{1,5},{5,9},{9,... | collective-permute-start | bytes 196616 | tf_op jit(solution)/shard_map/ppermute | solution.py:115
  17.3 120.7 %copy-start.3 = (f32[512,16]{0,1:T(8,128)}, f32[512,16]{0,1:T(8,128)S(1)}, u32[]{:S(2)}) copy-start(f32[512,16]{0,1:T(8,128)S(1)} %fusion.21) | copy-start | bytes 98308
  33.7 2.9 %copy-start.4 = (bf16[4,512]{1,0:T(4,128)(2,1)S(1)}, bf16[4,512]{1,0:T(4,128)(2,1)}, u32[]{:S(2)}) copy-start(bf16[4,512]{1,0:T(4,128)(2,1)} %param.21) | copy-start | bytes 12292
  33.7 2.9 %copy-start.5 = (bf16[4,512]{1,0:T(4,128)(2,1)S(1)}, bf16[4,512]{1,0:T(4,128)(2,1)}, u32[]{:S(2)}) copy-start(bf16[4,512]{1,0:T(4,128)(2,1)} %param.20) | copy-start | bytes 12292
  105.4 6.3 %copy-start.2 = (bf16[1,512,2048]{2,1,0:T(8,128)(2,1)S(1)}, bf16[1,512,2048]{2,1,0:T(8,128)(2,1)}, u32[]{:S(2)}) copy-start(bf16[1,512,2048]{2,1,0:T(8,128)(2,1)} %param.13) | copy-start | bytes 6291460
  125.0 10.5 %collective-permute-start.1 = (bf16[512,256]{1,0:T(8,128)(2,1)S(1)}, bf16[512,256]{1,0:T(8,128)(2,1)S(1)}, u32[]{:S(2)}, u32[]{:S(2)}) collective-permute-start(bf16[512,256]{1,0:T(8,128)(2,1)S(1)} %convert_element_type.49), channel_id=1, source_target_pairs={{0,4},{4,8},{8,12},{12,16},{16,20},{20,24},{24,28},{1,5},{5,9},{9,... | collective-permute-start | bytes 786440 | tf_op jit(solution)/shard_map/ppermute | solution.py:115
  136.7 12.8 %collective-permute-start.2 = (bf16[512,256]{1,0:T(8,128)(2,1)S(1)}, bf16[512,256]{1,0:T(8,128)(2,1)S(1)}, u32[]{:S(2)}, u32[]{:S(2)}) collective-permute-start(bf16[512,256]{1,0:T(8,128)(2,1)S(1)} %fusion.24), channel_id=1, source_target_pairs={{0,8},{4,12},{8,16},{12,20},{16,24},{20,28},{1,9},{5,13},{9,17},{1... | collective-permute-start | bytes 786440 | tf_op jit(solution)/shard_map/ppermute | solution.py:115
  142.3 7.2 %copy-start.1 = (f32[512,256]{1,0:T(8,128)S(1)}, f32[512,256]{1,0:T(8,128)}, u32[]{:S(2)}) copy-start(f32[512,256]{1,0:T(8,128)} %get-tuple-element.26) | copy-start | bytes 1572868
  149.7 26.1 %collective-permute-start.3 = (bf16[512,256]{1,0:T(8,128)(2,1)S(1)}, bf16[512,256]{1,0:T(8,128)(2,1)S(1)}, u32[]{:S(2)}, u32[]{:S(2)}) collective-permute-start(bf16[512,256]{1,0:T(8,128)(2,1)S(1)} %fusion.26), channel_id=1, source_target_pairs={{0,16},{4,20},{8,24},{12,28},{1,17},{5,21},{9,25},{13,29},{2,18},{... | collective-permute-start | bytes 786440 | tf_op jit(solution)/shard_map/ppermute | solution.py:115
Sparse Core Ops, SparseCore 0:
  10.2 95.1 all-gather.3
  108.3 68.6 all-gather.5
